TPU v7x, 512 devices: a whole 4x4x16 slice. The times are simulated.
512 devices in a mesh: gr: 2 (over z_hi), sp: 32 (over z_lo, y), tp: 8 (over x, core).
Axes of the slice: x: 4, y: 4, z: 16 (z_hi: 2, z_lo: 8; z = z_hi * 8 + z_lo), core: 2. Of those that a mesh axis runs over, the one named last changes fastest.
Arguments:
- tokens: bfloat16 [8, 4096, 4096], P('gr', 'sp'), parts along dimension 0, may hold values from -6 to 6
- key_weight: bfloat16 [4096, 2048], P('sp', 'tp'), may hold values from -0.09375 to 0.09375
- value_weight: bfloat16 [4096, 2048], P('sp', 'tp'), may hold values from -0.09375 to 0.09375
- log_decay: float32 [32, 8, 4096], P('tp', 'gr', 'sp'), parts along dimension 1, may hold values from -1 to 0, as said below
- new_query: bfloat16 [8, 2048], P('gr', 'tp'), parts along dimension 0, may hold values from -6 to 6
- new_key: bfloat16 [8, 2048], P('gr', 'tp'), parts along dimension 0, may hold values from -24 to 24
- new_value: bfloat16 [8, 2048], P('gr', 'tp'), parts along dimension 0, may hold values from -6 to 6
- step_decay: float32 [32, 8], P('tp', 'gr'), parts along dimension 1, may hold values from -1.5 to -0.05
- norm_gain: float32 [2048], P('tp'), may hold values from 0.1 to 1.9
Outputs:
- state_cache: float32 [512, 32, 64], P('gr', 'tp'), parts along dimension 0
- first_read: bfloat16 [8, 2048], P('gr', 'tp'), parts along dimension 0
There are 2 independent parts, one for each index of `gr`. A program takes and returns all parts, laid end to end along the dimension named above; an argument that names none is the same for every part. Nothing has to cross between parts.
Inputs may be any that keep to these rules, and one draw needn't show every extreme that they name: `log_decay`: every entry is at most zero.
All inputs are finite; a program needn't handle non-finite values.
Results may differ from a plain program's by a relative error of at most 0.0053.
Values may be sent and summed in bfloat16 or wider, within the bound.
No kernel may reach another device: no remote copies, remote signals or barrier semaphores. Data moves between devices by JAX's collectives and lax.ppermute only.
A program may use at most 64 MiB of HBM per device.

v0:
```python
import jax
import jax.numpy as jnp
from jax import lax
from jax.sharding import PartitionSpec as P

HEAD_DIM = 64


def in_one_piece(arrays, axis, dim, along):
    ends, at = ([], 0)
    for a in arrays[:-1]:
        at += a.shape[along]
        ends.append(at)
    both = jnp.concatenate(arrays, axis=along)
    return tuple(jnp.split(lax.all_gather(both, axis, axis=dim, tiled=True), ends, axis=along))


def copy_for_each(x, axis):
    devices = lax.axis_size(axis)
    return lax.all_to_all(jnp.broadcast_to(x[None], (devices, *x.shape)), axis, 0, 0, tiled=True)


def joined_by_halves(pieces, combine):
    while len(jax.tree.leaves(pieces)[0]) > 1:
        pieces = jax.vmap(combine)(*(pieces[side::2] for side in (0, 1)))
    return pieces[0]


def carried_in(x, axis, combine, identity):
    devices, mine = (lax.axis_size(axis), lax.axis_index(axis))
    passed = jnp.arange(devices) > mine

    def kept(part, zero, own):
        part = jnp.where(
            passed.reshape(-1, *(1 for _ in own.shape)), part, jnp.asarray(zero, own.dtype)
        )
        return part[::-1]

    pieces = copy_for_each(x, axis)
    return joined_by_halves(kept(pieces, identity, x), combine)


def cut_along(x, dim, devices):
    shape = x.shape
    blocks = x.reshape(*shape[:dim], devices, shape[dim] // devices, *shape[dim + 1 :])
    return jnp.moveaxis(blocks, dim, 0)


def sum_at_owner(x, axis, dim):
    blocks = cut_along(x, dim, lax.axis_size(axis))
    arrived = lax.all_to_all(blocks, axis, split_axis=0, concat_axis=0, tiled=True)
    return arrived.sum(axis=0)


def joined_along(blocks, dim):
    shape = list(blocks.shape[1:])
    shape[dim] *= blocks.shape[0]
    return jnp.moveaxis(blocks, 0, dim).reshape(shape)


def gather_directly(x, axis, dim):
    return joined_along(copy_for_each(x, axis), dim)


def rotate_half(values, positions):
    half = values.shape[-1] // 2
    inverse = 10000.0 ** (-jnp.arange(half, dtype=jnp.float32) * (2.0 / values.shape[-1]))
    angles = positions[..., None] * inverse
    cosine = jnp.cos(angles)
    sine = jnp.sin(angles)
    first, second = (values[..., :half], values[..., half:])
    return jnp.concatenate(
        [first * cosine - second * sine, second * cosine + first * sine], axis=-1
    )


def add_totals(earlier, later):
    return earlier + later


def shards(
    tokens,
    key_weight,
    value_weight,
    log_decay,
    new_query,
    new_key,
    new_value,
    step_decay,
    norm_gain,
):
    seqs, span, width = tokens.shape
    heads_here = key_weight.shape[1] // HEAD_DIM
    token_rows = tokens.reshape(seqs * span, width)
    whole_keys, whole_values = in_one_piece((key_weight, value_weight), "sp", 0, 1)
    key_sum = jnp.dot(token_rows, whole_keys, preferred_element_type=jnp.float32)
    value_sum = jnp.dot(token_rows, whole_values, preferred_element_type=jnp.float32)
    key_vectors = (
        lax.optimization_barrier(key_sum.astype(jnp.bfloat16))
        .astype(jnp.float32)
        .reshape(seqs, span, heads_here, HEAD_DIM)
    )
    values = (
        lax.optimization_barrier(value_sum.astype(jnp.bfloat16))
        .astype(jnp.float32)
        .reshape(seqs, span, heads_here, HEAD_DIM)
    )
    devices = lax.axis_size("sp")
    offset = lax.axis_index("sp") * span
    positions = (offset + jnp.arange(span, dtype=jnp.int32)).astype(jnp.float32)
    rkeys = rotate_half(key_vectors, positions[None, :, None]) * HEAD_DIM ** (-0.5)
    totals = jnp.sum(log_decay, axis=-1)
    later_sum = carried_in(totals, "sp", add_totals, jnp.zeros_like(totals))
    weight = jnp.exp(totals[:, :, None] - jnp.cumsum(log_decay, axis=-1) + later_sum[:, :, None])
    weighted = rkeys * jnp.transpose(weight, (1, 2, 0))[:, :, :, None]
    term = jnp.einsum("stha,sthb->sahb", weighted, values, precision=lax.Precision.HIGHEST)
    term = term.reshape(seqs * HEAD_DIM, heads_here, HEAD_DIM)
    end_pos = jnp.full((seqs, heads_here), float(span * devices), jnp.float32)
    query = rotate_half(new_query.astype(jnp.float32).reshape(seqs, heads_here, HEAD_DIM), end_pos)
    key_new = rotate_half(
        new_key.astype(jnp.float32).reshape(seqs, heads_here, HEAD_DIM), end_pos
    ) * HEAD_DIM ** (-0.5)
    value_new = new_value.astype(jnp.float32).reshape(seqs, heads_here, HEAD_DIM)
    decay_all = jnp.repeat(jnp.exp(step_decay).T, HEAD_DIM, axis=0)
    key_all = jnp.transpose(key_new, (0, 2, 1)).reshape(seqs * HEAD_DIM, heads_here)
    value_all = jnp.repeat(value_new, HEAD_DIM, axis=0)
    rows = seqs * HEAD_DIM // devices
    owned = sum_at_owner(term, "sp", 0)
    first_row = lax.axis_index("sp") * rows
    decay_rows = lax.dynamic_slice_in_dim(decay_all, first_row, rows, 0)
    key_rows = lax.dynamic_slice_in_dim(key_all, first_row, rows, 0)
    value_rows = lax.dynamic_slice_in_dim(value_all, first_row, rows, 0)
    finished = decay_rows[:, :, None] * owned + key_rows[:, :, None] * value_rows
    state_cache = gather_directly(finished, "sp", 0)
    state_seq = state_cache.reshape(seqs, HEAD_DIM, heads_here, HEAD_DIM)
    raw = jnp.einsum("sha,sahb->shb", query, state_seq, precision=lax.Precision.HIGHEST)
    center = jnp.mean(raw, axis=-1, keepdims=True)
    spread = jnp.mean(jnp.square(raw - center), axis=-1, keepdims=True)
    normed = (raw - center) * lax.rsqrt(spread + 1e-06) * norm_gain.reshape(heads_here, HEAD_DIM)
    first_read = normed.reshape(seqs, heads_here * HEAD_DIM).astype(jnp.bfloat16)
    return (state_cache, first_read)


def solution(mesh):
    placed = (
        P("gr", "sp", None),
        P("sp", "tp"),
        P("sp", "tp"),
        P("tp", "gr", "sp"),
        P("gr", "tp"),
        P("gr", "tp"),
        P("gr", "tp"),
        P("tp", "gr"),
        P("tp"),
    )
    return jax.shard_map(
        shards,
        mesh=mesh,
        in_specs=placed,
        out_specs=(P("gr", "tp", None), P("gr", "tp")),
        check_vma=False,
    )
```

profile of v0, /device:TPU:4, one launch (start us, length us, event | category | flops | bytes accessed | tf_op | source)
XLA Modules:
  0.0 318.0 jit_solution(11815697062888992567)
XLA Ops:
  7.2 0.0 all-gather.2.cloned.1.call-start
  7.2 1.5 pad_maximum_fusion
  8.7 0.0 all-gather.2.cloned.1.call-update
  8.8 0.8 reduce_sum.36
  9.6 0.6 broadcast_in_dim.22
  10.2 15.5 %all-to-all-start = ((f32[32,4,4]{2,1,0:T(4,128)}), f32[32,4,4]{2,1,0:T(4,128)S(1)}, u32[]{:S(2)}, u32[]{:S(2)}) async-start(f32[32,4,4]{2,1,0:T(4,128)} %broadcast_in_dim.22), calls=%async_computation | async-start | bytes 131072 | tf_op jit(solution)/shard_map/all_to_all | solution.py:20
  25.8 0.7 exponential_bitcast_fusion
  26.5 0.1 multiply_cosine_fusion
  26.6 2.3 reduce_window_sum.13
  28.9 9.8 %all-to-all-done = f32[32,4,4]{2,1,0:T(4,128)S(1)} async-done(((f32[32,4,4]{2,1,0:T(4,128)}), f32[32,4,4]{2,1,0:T(4,128)S(1)}, u32[]{:S(2)}, u32[]{:S(2)}) %all-to-all-start) | async-done | bytes 2080 | tf_op jit(solution)/shard_map/all_to_all | solution.py:20
  38.7 0.1 broadcast_select_fusion
  38.9 0.1 fusion.25
  39.0 203.1 %all-gather.2.cloned.1.call-done = bf16[4096,512]{1,0:T(8,128)(2,1)} async-done(((bf16[128,512]{1,0:T(8,128)(2,1)}), bf16[4096,512]{1,0:T(8,128)(2,1)}) %all-gather.2.cloned.1.call-update) | async-done | bytes 4194320 | tf_op jit(solution)/shard_map/all_gather | solution.py:15
  242.2 4.1 %fusion.13 = bf16[512,256]{0,1:T(8,128)(2,1)S(1)} fusion(bf16[512,4096]{1,0:T(8,128)(2,1)} %bitcast.61, bf16[4096,512]{1,0:T(8,128)(2,1)} %all-gather.2.cloned.1.call-done), kind=kOutput, calls=%fused_computation.8 | convolution fusion | flops 1073872896 | bytes 6553600 | tf_op jit(solution)/shard_map/dot_general | solution.py:97
  246.3 0.1 reshape.156
  246.4 4.1 %fusion.10 = bf16[512,256]{0,1:T(8,128)(2,1)S(1)} fusion(bf16[512,4096]{1,0:T(8,128)(2,1)} %bitcast.62, bf16[4096,512]{1,0:T(8,128)(2,1)} %all-gather.2.cloned.1.call-done), kind=kOutput, calls=%fused_computation.7 | convolution fusion | flops 1073872896 | bytes 6553600 | tf_op jit(solution)/shard_map/dot_general | solution.py:96
  250.5 0.0 copy-start
  250.5 0.0 copy-start.1
  250.5 0.0 copy-start.2
  250.5 0.2 reshape.169
  250.7 0.1 multiply_subtract_fusion
  250.8 0.6 convolution_bitcast_fusion
  251.4 0.0 copy-start.3
  251.4 0.2 copy.31
  251.6 0.1 copy.71
  251.7 1.0 reshape.178
  252.7 11.9 %all-to-all-start.1 = ((f32[32,1,2048]{2,1,0:T(1,128)}), f32[32,1,2048]{2,1,0:T(1,128)S(1)}, u32[]{:S(2)}, u32[]{:S(2)}) async-start(f32[32,1,2048]{2,1,0:T(1,128)} %reshape.178), calls=%async_computation.1 | async-start | bytes 524288 | tf_op jit(solution)/shard_map/all_to_all | solution.py:51
  264.6 0.1 broadcast_in_dim.20
  264.7 0.1 reshape.154
  264.8 0.0 copy-done
  264.8 0.1 reshape.175
  264.9 0.0 copy-done.1
  264.9 0.1 reshape.171
  265.0 0.0 copy-done.2
  265.0 0.1 reshape.173
  265.1 0.1 multiply_sine_fusion.1
  265.1 0.1 fusion.33
  265.2 0.1 fusion.32
  265.3 0.1 fusion.22
  265.4 0.1 reshape.161
  265.5 0.1 constant_dynamic-slice_fusion
  265.5 17.9 %all-to-all-done.1 = f32[32,1,2048]{2,1,0:T(1,128)S(1)} async-done(((f32[32,1,2048]{2,1,0:T(1,128)}), f32[32,1,2048]{2,1,0:T(1,128)S(1)}, u32[]{:S(2)}, u32[]{:S(2)}) %all-to-all-start.1) | async-done | bytes 262176 | tf_op jit(solution)/shard_map/all_to_all | solution.py:51
  283.4 0.5 broadcast.128
  283.9 1.3 reduce
  285.2 0.2 reshape.179
  285.4 0.1 bitcast_reduce_fusion
  285.5 0.1 multiply_add_fusion.1
  285.6 0.1 broadcast_bitcast_fusion
  285.7 1.0 reshape.180
  286.7 5.5 %all-to-all-start.2 = ((f32[32,1,2048]{2,1,0:T(1,128)}), f32[32,1,2048]{2,1,0:T(1,128)S(1)}, u32[]{:S(2)}, u32[]{:S(2)}) async-start(f32[32,1,2048]{2,1,0:T(1,128)} %reshape.180), calls=%async_computation.2 | async-start | bytes 524288 | tf_op jit(solution)/shard_map/all_to_all | solution.py:20
  292.2 0.0 copy-done.3
  292.2 0.1 mul.218
  292.3 0.1 maximum_bitcast_fusion
  292.4 14.8 %all-to-all-done.2 = f32[32,1,2048]{2,1,0:T(1,128)S(1)} async-done(((f32[32,1,2048]{2,1,0:T(1,128)}), f32[32,1,2048]{2,1,0:T(1,128)S(1)}, u32[]{:S(2)}, u32[]{:S(2)}) %all-to-all-start.2) | async-done | bytes 262176 | tf_op jit(solution)/shard_map/all_to_all | solution.py:20
  307.2 1.3 reduce.1
  308.5 0.2 reshape.181
  308.7 0.1 fusion.29
  308.8 0.5 fusion.18
  309.3 0.1 reduce_sum.38
  309.4 0.2 multiply_reduce_fusion
  309.6 0.1 multiply_convert_fusion
  309.6 0.7 convert_element_type.36
  310.3 0.9 copy.40
  (17 shorter events, 0.2 us)
Async XLA Ops:
  7.2 235.0 %all-gather.2.cloned.1.call-start = ((), (), s32[]{:S(2)}) async-start(), calls=%async_computation.3 | async-start | bytes 4325376 | tf_op jit(solution)/shard_map/all_gather | solution.py:15
  10.2 28.5 %all-to-all-start = ((f32[32,4,4]{2,1,0:T(4,128)}), f32[32,4,4]{2,1,0:T(4,128)S(1)}, u32[]{:S(2)}, u32[]{:S(2)}) async-start(f32[32,4,4]{2,1,0:T(4,128)} %broadcast_in_dim.22), calls=%async_computation | async-start | bytes 131072 | tf_op jit(solution)/shard_map/all_to_all | solution.py:20
  250.5 14.3 %copy-start = (bf16[4,256]{1,0:T(4,128)(2,1)S(1)}, bf16[4,256]{1,0:T(4,128)(2,1)}, u32[]{:S(2)}) copy-start(bf16[4,256]{1,0:T(4,128)(2,1)} %param.13) | copy-start | bytes 6148
  250.5 14.4 %copy-start.1 = (bf16[4,256]{1,0:T(4,128)(2,1)S(1)}, bf16[4,256]{1,0:T(4,128)(2,1)}, u32[]{:S(2)}) copy-start(bf16[4,256]{1,0:T(4,128)(2,1)} %param.14) | copy-start | bytes 6148
  250.5 14.5 %copy-start.2 = (bf16[4,256]{1,0:T(4,128)(2,1)S(1)}, bf16[4,256]{1,0:T(4,128)(2,1)}, u32[]{:S(2)}) copy-start(bf16[4,256]{1,0:T(4,128)(2,1)} %param.15) | copy-start | bytes 6148
  251.4 40.8 %copy-start.3 = (f32[256]{0:T(256)S(1)}, f32[256]{0:T(256)}, u32[]{:S(2)}) copy-start(f32[256]{0:T(256)} %param.17) | copy-start | bytes 3076
  252.7 30.7 %all-to-all-start.1 = ((f32[32,1,2048]{2,1,0:T(1,128)}), f32[32,1,2048]{2,1,0:T(1,128)S(1)}, u32[]{:S(2)}, u32[]{:S(2)}) async-start(f32[32,1,2048]{2,1,0:T(1,128)} %reshape.178), calls=%async_computation.1 | async-start | bytes 524288 | tf_op jit(solution)/shard_map/all_to_all | solution.py:51
  286.7 20.5 %all-to-all-start.2 = ((f32[32,1,2048]{2,1,0:T(1,128)}), f32[32,1,2048]{2,1,0:T(1,128)S(1)}, u32[]{:S(2)}, u32[]{:S(2)}) async-start(f32[32,1,2048]{2,1,0:T(1,128)} %reshape.180), calls=%async_computation.2 | async-start | bytes 524288 | tf_op jit(solution)/shard_map/all_to_all | solution.py:20
Sparse Core Ops, SparseCore 0:
  10.6 231.4 all-gather.1
where the time goes:
time: 319 us; the launch traced here: 318 us
  waiting for transfers between devices  246 us (77%)
  starting transfers between devices  32.9 us (10%)
  between operations  14.3 us (4%)
  matrix products  9.31 us (3%)
  other arithmetic  8.33 us (3%)
  local copies, waits for them, and re-layouts  7.42 us (2%)
    all_gather x1, waiting for transfers between devices, in_one_piece(): lax.all_gather(both, axis, axis=dim, tiled=True)  203 us
    all_to_all x2, waiting for transfers between devices, copy_for_each(): lax.all_to_all(jnp.broadcast_to(x[None], (devices, *x.shape)), axis, 0, 0...  24.6 us
    all_to_all x2, starting transfers between devices, copy_for_each(): lax.all_to_all(jnp.broadcast_to(x[None], (devices, *x.shape)), axis, 0, 0...  21 us
    all_to_all x1, waiting for transfers between devices, sum_at_owner(): lax.all_to_all(blocks, axis, split_axis=0, concat_axis=0, tiled=True)  17.9 us
    all_to_all x1, starting transfers between devices, sum_at_owner(): lax.all_to_all(blocks, axis, split_axis=0, concat_axis=0, tiled=True)  11.9 us
  transfers between devices with their start and end apart: 4, of which 4 were waited for; matrix products, arithmetic and copies ran while one was open for 2% of the time, Pallas kernels for 0%

commit v1 on v0

--- a/solution.py
+++ b/solution.py
@@ -92,7 +92,13 @@
     seqs, span, width = tokens.shape
     heads_here = key_weight.shape[1] // HEAD_DIM
     token_rows = tokens.reshape(seqs * span, width)
-    whole_keys, whole_values = in_one_piece((key_weight, value_weight), "sp", 0, 1)
+    depth = key_weight.shape[0]
+    half = depth // lax.axis_size("gr")
+    both = jnp.concatenate([key_weight, value_weight], axis=1)
+    mine = lax.dynamic_slice_in_dim(both, lax.axis_index("gr") * half, half, 0)
+    got = lax.all_gather(mine, ("gr", "sp"), axis=0, tiled=False)
+    got = jnp.moveaxis(got.reshape(2, 32, half, both.shape[1]), 0, 1).reshape(32 * depth, -1)
+    whole_keys, whole_values = jnp.split(got, 2, axis=1)
     key_sum = jnp.dot(token_rows, whole_keys, preferred_element_type=jnp.float32)
     value_sum = jnp.dot(token_rows, whole_values, preferred_element_type=jnp.float32)
     key_vectors = (

time: 319 us -> 228 us (0.71)
  the two profiles are of different devices: /device:TPU:4 before, /device:TPU:2 now
where the time goes in v1:
time: 228 us; the launch traced here: 227 us
  waiting for transfers between devices  162 us (71%)
  starting transfers between devices  28.3 us (12%)
  between operations  14.4 us (6%)
  local copies, waits for them, and re-layouts  10.9 us (5%)
  other arithmetic  8.17 us (4%)
  matrix products  3.67 us (2%)
    all_gather x1, waiting for transfers between devices, shards(): got = lax.all_gather(mine, ('gr', 'sp'), axis=0, tiled=False)  123 us
    all_to_all x2, waiting for transfers between devices, copy_for_each(): lax.all_to_all(jnp.broadcast_to(x[None], (devices, *x.shape)), axis, 0, 0...  24.4 us
    all_to_all x2, starting transfers between devices, copy_for_each(): lax.all_to_all(jnp.broadcast_to(x[None], (devices, *x.shape)), axis, 0, 0...  21 us
    all_to_all x1, waiting for transfers between devices, sum_at_owner(): lax.all_to_all(blocks, axis, split_axis=0, concat_axis=0, tiled=True)  14.2 us
    all_to_all x1, starting transfers between devices, sum_at_owner(): lax.all_to_all(blocks, axis, split_axis=0, concat_axis=0, tiled=True)  7.31 us
  transfers between devices with their start and end apart: 4, of which 4 were waited for; matrix products, arithmetic and copies ran while one was open for 3% of the time, Pallas kernels for 0%

profile of v1, /device:TPU:2, one launch (start us, length us, event | category | flops | bytes accessed | tf_op | source)
XLA Modules:
  0.0 227.4 jit_solution(16160083685254658363)
XLA Ops:
  7.2 0.0 all-gather.3.cloned.1.call-start
  7.2 1.4 fusion.22
  8.6 0.0 all-gather.3.cloned.1.call-update
  8.7 0.8 reduce_sum.36
  9.4 0.6 broadcast_in_dim.22
  10.1 15.5 %all-to-all-start = ((f32[32,4,4]{2,1,0:T(4,128)}), f32[32,4,4]{2,1,0:T(4,128)S(1)}, u32[]{:S(2)}, u32[]{:S(2)}) async-start(f32[32,4,4]{2,1,0:T(4,128)} %broadcast_in_dim.22), calls=%async_computation | async-start | bytes 131072 | tf_op jit(solution)/shard_map/all_to_all | solution.py:20
  25.6 0.8 reshape.183
  26.4 0.1 fusion.33
  26.5 0.1 multiply_cosine_fusion
  26.7 2.3 reduce_window_sum.13
  28.9 9.6 %all-to-all-done = f32[32,4,4]{2,1,0:T(4,128)S(1)} async-done(((f32[32,4,4]{2,1,0:T(4,128)}), f32[32,4,4]{2,1,0:T(4,128)S(1)}, u32[]{:S(2)}, u32[]{:S(2)}) %all-to-all-start) | async-done | bytes 2080 | tf_op jit(solution)/shard_map/all_to_all | solution.py:20
  38.5 0.1 broadcast_select_fusion
  38.7 0.1 fusion.26
  38.8 123.4 %all-gather.3.cloned.1.call-done = bf16[4096,512]{1,0:T(8,128)(2,1)} async-done(((bf16[64,512]{1,0:T(8,128)(2,1)}), bf16[4096,512]{1,0:T(8,128)(2,1)}) %all-gather.3.cloned.1.call-update) | async-done | bytes 4194320 | tf_op jit(solution)/shard_map/all_gather | solution.py:99
  162.2 0.0 copy-start.4
  162.2 2.8 %copy.39 = bf16[32,2,64,512]{3,2,1,0:T(8,128)(2,1)S(1)} copy(bf16[32,2,64,512]{3,2,0,1:T(8,128)(2,1)} %bitcast.57) | data formatting | bytes 8388608 | tf_op jit(solution)/shard_map/transpose | solution.py:100
  165.0 0.6 copy-done.4
  165.6 1.3 fusion.10
  166.9 1.3 fusion.13
  168.3 0.0 copy-start
  168.3 0.0 copy-start.2
  168.3 0.0 copy-start.1
  168.3 0.2 reshape.177
  168.5 0.1 reshape.164
  168.6 0.1 multiply_subtract_fusion
  168.7 0.6 convolution_bitcast_fusion
  169.2 0.0 copy-start.3
  169.2 0.2 copy.44
  169.4 0.1 copy.84
  169.5 1.0 reshape.188
  170.5 7.3 %all-to-all-start.1 = ((f32[32,1,2048]{2,1,0:T(1,128)}), f32[32,1,2048]{2,1,0:T(1,128)S(1)}, u32[]{:S(2)}, u32[]{:S(2)}) async-start(f32[32,1,2048]{2,1,0:T(1,128)} %reshape.188), calls=%async_computation.1 | async-start | bytes 524288 | tf_op jit(solution)/shard_map/all_to_all | solution.py:51
  177.9 0.0 copy-done
  177.9 0.1 reshape.179
  178.0 0.1 fusion.34
  178.1 0.1 fusion.23
  178.2 0.1 reshape.169
  178.3 0.0 copy-done.2
  178.3 0.1 broadcast_in_dim.20
  178.4 0.1 reshape.160
  178.5 0.0 copy-done.1
  178.5 0.1 reshape.181
  178.6 0.1 constant_dynamic-slice_fusion
  178.6 14.2 %all-to-all-done.1 = f32[32,1,2048]{2,1,0:T(1,128)S(1)} async-done(((f32[32,1,2048]{2,1,0:T(1,128)}), f32[32,1,2048]{2,1,0:T(1,128)S(1)}, u32[]{:S(2)}, u32[]{:S(2)}) %all-to-all-start.1) | async-done | bytes 262176 | tf_op jit(solution)/shard_map/all_to_all | solution.py:51
  192.8 0.5 broadcast.128
  193.4 1.3 reduce
  194.6 0.2 reshape.189
  194.8 0.1 bitcast_reduce_fusion
  194.9 0.1 multiply_add_fusion.1
  195.0 0.1 broadcast_bitcast_fusion
  195.1 1.0 reshape.190
  196.1 5.5 %all-to-all-start.2 = ((f32[32,1,2048]{2,1,0:T(1,128)}), f32[32,1,2048]{2,1,0:T(1,128)S(1)}, u32[]{:S(2)}, u32[]{:S(2)}) async-start(f32[32,1,2048]{2,1,0:T(1,128)} %reshape.190), calls=%async_computation.2 | async-start | bytes 524288 | tf_op jit(solution)/shard_map/all_to_all | solution.py:20
  201.6 0.0 copy-done.3
  201.6 0.1 mul.222
  201.7 0.1 maximum_bitcast_fusion
  201.7 14.8 %all-to-all-done.2 = f32[32,1,2048]{2,1,0:T(1,128)S(1)} async-done(((f32[32,1,2048]{2,1,0:T(1,128)}), f32[32,1,2048]{2,1,0:T(1,128)S(1)}, u32[]{:S(2)}, u32[]{:S(2)}) %all-to-all-start.2) | async-done | bytes 262176 | tf_op jit(solution)/shard_map/all_to_all | solution.py:20
  216.6 1.3 reduce.1
  217.8 0.2 reshape.191
  218.1 0.1 fusion.30
  218.1 0.5 fusion.18
  218.6 0.1 reduce_sum.38
  218.7 0.2 multiply_reduce_fusion
  218.9 0.1 multiply_convert_fusion
  219.0 0.7 convert_element_type.36
  219.7 0.9 copy.53
  (19 shorter events, 0.3 us)
Async XLA Ops:
  7.2 155.0 %all-gather.3.cloned.1.call-start = ((), (), s32[]{:S(2)}) async-start(), calls=%async_computation.3 | async-start | bytes 4259840 | tf_op jit(solution)/shard_map/all_gather | solution.py:99
  10.1 28.4 %all-to-all-start = ((f32[32,4,4]{2,1,0:T(4,128)}), f32[32,4,4]{2,1,0:T(4,128)S(1)}, u32[]{:S(2)}, u32[]{:S(2)}) async-start(f32[32,4,4]{2,1,0:T(4,128)} %broadcast_in_dim.22), calls=%async_computation | async-start | bytes 131072 | tf_op jit(solution)/shard_map/all_to_all | solution.py:20
  162.2 3.4 %copy-start.4 = (bf16[4,128,4096]{2,1,0:T(8,128)(2,1)S(1)}, bf16[4,128,4096]{2,1,0:T(8,128)(2,1)}, u32[]{:S(2)}) copy-start(bf16[4,128,4096]{2,1,0:T(8,128)(2,1)} %param.9) | copy-start | bytes 12582916
  168.3 9.6 %copy-start = (bf16[4,256]{1,0:T(4,128)(2,1)S(1)}, bf16[4,256]{1,0:T(4,128)(2,1)}, u32[]{:S(2)}) copy-start(bf16[4,256]{1,0:T(4,128)(2,1)} %param.14) | copy-start | bytes 6148
  168.3 10.0 %copy-start.2 = (f32[4,4]{1,0:T(4,128)S(1)}, f32[4,4]{1,0:T(4,128)}, u32[]{:S(2)}) copy-start(f32[4,4]{1,0:T(4,128)} %param.16) | copy-start | bytes 196
  168.3 10.2 %copy-start.1 = (bf16[4,256]{1,0:T(4,128)(2,1)S(1)}, bf16[4,256]{1,0:T(4,128)(2,1)}, u32[]{:S(2)}) copy-start(bf16[4,256]{1,0:T(4,128)(2,1)} %param.15) | copy-start | bytes 6148
  169.2 32.4 %copy-start.3 = (f32[256]{0:T(256)S(1)}, f32[256]{0:T(256)}, u32[]{:S(2)}) copy-start(f32[256]{0:T(256)} %param.17) | copy-start | bytes 3076
  170.5 22.3 %all-to-all-start.1 = ((f32[32,1,2048]{2,1,0:T(1,128)}), f32[32,1,2048]{2,1,0:T(1,128)S(1)}, u32[]{:S(2)}, u32[]{:S(2)}) async-start(f32[32,1,2048]{2,1,0:T(1,128)} %reshape.188), calls=%async_computation.1 | async-start | bytes 524288 | tf_op jit(solution)/shard_map/all_to_all | solution.py:51
  196.1 20.4 %all-to-all-start.2 = ((f32[32,1,2048]{2,1,0:T(1,128)}), f32[32,1,2048]{2,1,0:T(1,128)S(1)}, u32[]{:S(2)}, u32[]{:S(2)}) async-start(f32[32,1,2048]{2,1,0:T(1,128)} %reshape.190), calls=%async_computation.2 | async-start | bytes 524288 | tf_op jit(solution)/shard_map/all_to_all | solution.py:20
Sparse Core Ops, SparseCore 0:
  11.5 150.6 all-gather.2
